TPU v7x, 32 devices: a whole 2x2x4 slice. The times are simulated.
32 devices in a mesh: grp: 2 (over y), fs: 4 (over z), tp: 4 (over x, core).
Axes of the slice: x: 2, y: 2, z: 4, core: 2. Of those that a mesh axis runs over, the one named last changes fastest.
Arguments:
- tokens: bfloat16 [8192, 2048], P(('grp', 'fs'), 'tp'), parts along dimension 0, may hold values from -50 to 50
- mix_gain: float32 [2048], replicated, may hold values from 0.1 to 1.9
- value_proj: bfloat16 [2048, 1024], P('fs', 'tp'), may hold values from -0.125 to 0.125
- gate_proj: bfloat16 [2048, 1024], P('fs', 'tp'), may hold values from -0.125 to 0.125
- conv_taps: float32 [31, 1024], P(None, 'tp'), may hold values from -1 to 1
- chan_gain: float32 [1024], replicated, may hold values from 0.1 to 1.9
- chan_shift: float32 [1024], replicated, may hold values from -3 to 3
- mix_out: bfloat16 [1024, 2048], P('fs', 'tp'), may hold values from -0.1875 to 0.1875
- mlp_gain: float32 [2048], replicated, may hold values from 0.1 to 1.9
- mlp_gate: bfloat16 [2048, 5632], P('fs', 'tp'), may hold values from -0.125 to 0.125
- mlp_up: bfloat16 [2048, 5632], P('fs', 'tp'), may hold values from -0.125 to 0.125
- gate_taps: float32 [3, 5632], P(None, 'tp'), may hold values from -3.5 to 3.5
- up_taps: float32 [3, 5632], P(None, 'tp'), may hold values from -3.5 to 3.5
- mlp_down: bfloat16 [5632, 2048], P('tp', 'fs'), may hold values from -0.078125 to 0.078125
- final_gain: float32 [2048], P('tp'), may hold values from 0.1 to 1.9
Outputs:
- layer_out: bfloat16 [8192, 2048], P(('grp', 'fs'), 'tp'), parts along dimension 0
There are 2 independent parts, one for each index of `grp`. A program takes and returns all parts, laid end to end along the dimension named above; an argument that names none is the same for every part. Nothing has to cross between parts.
All inputs are finite; a program needn't handle non-finite values.
Results may differ from a plain program's by a relative error of at most 0.0095.
Values may be sent and summed in bfloat16 or wider, within the bound.
A program may use at most 128 MiB of HBM per device.

v0:
```python
import functools
from types import SimpleNamespace

import jax
import jax.numpy as jnp
from jax import lax
from jax.experimental import pallas as pl
from jax.experimental.pallas import tpu as pltpu
from jax.sharding import PartitionSpec as P

MESH = pl.DeviceIdType.MESH
F32, BF16 = jnp.float32, jnp.bfloat16
LANES = 128
CORES = 2
LEAD = 2
PAD = 16
EDGE = 8
BUDGET = 4.5


def column_chunks(width, most):
    return [(first, min(most, width - first)) for first in range(0, width, most)]


def sigmoid(value):
    return 1.0 / (1.0 + jnp.exp(-value))


def layer_kernel(n, *refs):
    arrays = SimpleNamespace(**dict(zip(n.inputs, refs)))
    out = refs[len(n.inputs)]
    s = SimpleNamespace(**dict(zip(n.scratch, refs[len(n.inputs) + 1 :])))

    group, fs, tp = lax.axis_index("grp"), lax.axis_index("fs"), lax.axis_index("tp")
    chip, core = tp // CORES, tp % CORES
    sibling = tp + 1 - 2 * core

    def chip_at(jump):
        return (chip + jump + n.chips) % n.chips

    def rows_of(r):
        return pl.ds(r * n.rows, n.rows)

    local = {}

    def load(name, src, dst):
        index = len(local)
        local[name] = pltpu.make_async_copy(src, dst, s.local_sem.at[index])
        local[name].start()

    loaded = set()

    def have(*names):
        for name in names:
            if name not in loaded:
                loaded.add(name)
                local[name].wait()

    def own_rows(dst, count):
        return dst.at[pl.ds(pl.multiple_of(fs * count, count), count), :]

    load("tokens", arrays.tokens, s.tok.at[tp])
    for name in n.small:
        load(name, getattr(arrays, name), getattr(s, "v_" + name))
    load("value", arrays.value, own_rows(s.wv, n.depth))
    load("gate", arrays.gate, own_rows(s.wg, n.depth))
    load("mix", arrays.mix, own_rows(s.wm, n.mix_depth))
    load("mgate", arrays.mgate, own_rows(s.wgate, n.depth))
    load("mup", arrays.mup, own_rows(s.wup, n.depth))
    load("down", arrays.down, s.wd.at[fs])

    chunks = [
        (arrays.value, s.wv, n.depth, 0, n.own_channels),
        (arrays.gate, s.wg, n.depth, 0, n.own_channels),
        (arrays.mix, s.wm, n.mix_depth, 0, n.cols),
    ]
    first_mlp = len(chunks)
    for first, width in n.mlp_cols:
        chunks.append((arrays.mgate, s.wgate, n.depth, first, width))
        chunks.append((arrays.mup, s.wup, n.depth, first, width))
    first_down = len(chunks)
    for j in range(n.down_blocks):
        chunks.append((arrays.down, s.wd, n.hidden, j * LANES, LANES))
    assert len(chunks) == n.chunks

    def slot(i, f, part):
        _, dst, depth, first, width = chunks[i]
        half = depth // n.groups
        columns = pl.ds(first, width)
        if i >= first_down:
            return dst.at[f, pl.ds(pl.multiple_of(part * half, half), half), columns]
        return dst.at[pl.ds(pl.multiple_of(f * depth + part * half, half), half), columns]

    def z_copy(i, f, to, sems, own=False):
        src = slot(i, f, group)
        if own:
            source, _, depth, first, width = chunks[i]
            half = depth // n.groups
            src = source.at[pl.ds(pl.multiple_of(group * half, half), half), pl.ds(first, width)]
        return pltpu.make_async_remote_copy(
            src_ref=src,
            dst_ref=slot(i, f, group),
            send_sem=sems.at[i, f],
            recv_sem=s.z_recv.at[i, f],
            device_id={"fs": to},
            device_id_type=MESH,
        )

    def y_copy(i, f, jump, part):
        return pltpu.make_async_remote_copy(
            src_ref=slot(i, f, part),
            dst_ref=slot(i, f, part),
            send_sem=s.y_send.at[jump - 1, i, f],
            recv_sem=s.y_recv.at[jump - 1, i, f],
            device_id={"grp": (group + jump) % n.groups},
            device_id_type=MESH,
        )

    last = n.shards - 1
    reach = jnp.minimum(fs, last - fs)

    def arrival(step):
        near = fs - (step + 1) // 2 if step % 2 else fs + (step + 1) // 2
        distance = step - reach
        far = jnp.where(fs > last - fs, fs - distance, fs + distance)
        return jnp.where(step <= 2 * reach, near, far)

    def send_own(i):
        @pl.when(fs < last)
        def _():
            z_copy(i, fs, fs + 1, s.up_send, own=True).start()

        @pl.when(fs > 0)
        def _():
            z_copy(i, fs, fs - 1, s.down_send, own=True).start()

    def pump(i, step):
        f = arrival(step)
        z_copy(i, f, fs, s.up_send).wait_recv()

        @pl.when(jnp.logical_and(f < fs, fs < last))
        def _():
            z_copy(i, f, fs + 1, s.up_send).start()

        @pl.when(jnp.logical_and(f > fs, fs > 0))
        def _():
            z_copy(i, f, fs - 1, s.down_send).start()

        for jump in range(1, n.groups):
            y_copy(i, f, jump, group).start()

    def wait_y(i, f):
        for jump in range(1, n.groups):
            y_copy(i, f, jump, (group - jump + n.groups) % n.groups).wait_recv()

    def ready(i):
        for step in range(1, n.shards):
            wait_y(i, arrival(step))

    def drain_chunk(i):
        @pl.when(fs < last)
        def _():
            z_copy(i, fs, fs + 1, s.up_send, own=True).wait_send()

        @pl.when(fs > 0)
        def _():
            z_copy(i, fs, fs - 1, s.down_send, own=True).wait_send()

        for step in range(1, n.shards):
            f = arrival(step)

            @pl.when(jnp.logical_and(f < fs, fs < last))
            def _():
                z_copy(i, f, fs + 1, s.up_send).wait_send()

            @pl.when(jnp.logical_and(f > fs, fs > 0))
            def _():
                z_copy(i, f, fs - 1, s.down_send).wait_send()

            for jump in range(1, n.groups):
                y_copy(i, f, jump, group).wait_send()

    class Gather:
        def __init__(self, blocks, kind, own=None):
            self.blocks, self.kind, self.own = blocks, kind, own

        def copy(self, block, r, to, send, src=None):
            dst = self.blocks.at[block, rows_of(r), :]
            return pltpu.make_async_remote_copy(
                src_ref=dst if src is None else src,
                dst_ref=dst,
                send_sem=s.gather_send.at[self.kind, send, r],
                recv_sem=s.gather_recv.at[self.kind, block, r],
                device_id={"tp": to},
                device_id_type=MESH,
            )

        def own_copies(self, r):
            src = None if self.own is None else self.own.at[rows_of(r), :]
            copies = [
                self.copy(tp, r, chip_at(jump) * CORES + core, jump, src)
                for jump in range(1, n.chips)
            ]
            return copies + [self.copy(tp, r, sibling, 0, src)]

        def passed(self, r, jump):
            block = chip_at(-jump) * CORES + core
            return self.copy(block, r, sibling, n.chips - 1 + jump)

        def send(self, r):
            for copy in self.own_copies(r):
                copy.start()

        def forward(self, r):
            for jump in range(1, n.chips):
                copy = self.passed(r, jump)
                copy.wait_recv()
                copy.start()

        def wait(self, r):
            self.copy(sibling, r, sibling, 0).wait_recv()
            for jump in range(1, n.chips):
                block = chip_at(-jump) * CORES + 1 - core
                self.copy(block, r, sibling, 0).wait_recv()

        def drain(self, r):
            for copy in self.own_copies(r):
                copy.wait_send()
            for jump in range(1, n.chips):
                self.passed(r, jump).wait_send()

    tok = Gather(s.tok, 0, arrays.tokens)
    cv = Gather(s.cv, 1)
    mx = Gather(s.mx, 2)

    def each_tile(r, size, body):
        def step(q, carry):
            body(pl.multiple_of(r * n.rows + q * size, size))
            return carry

        lax.fori_loop(0, n.rows // size, step, 0)

    def norm_rows(blocks, gain, r):
        def body(first):
            rows = pl.ds(first, 32)
            total = jnp.zeros((32, 1), F32)
            for t in range(n.tps):
                v = blocks[t, rows, :].astype(F32)
                total = total + jnp.sum(v * v, axis=-1, keepdims=True)
            scale = lax.rsqrt(total / n.width + 1e-06)
            for t in range(n.tps):
                columns = slice(t * n.cols, (t + 1) * n.cols)
                v = blocks[t, rows, :].astype(F32)
                s.xn[rows, columns] = (v * scale * gain[:, columns]).astype(BF16)

        each_tile(r, 32, body)

    def dot(a, b):
        return jnp.dot(a, b, preferred_element_type=F32)

    def norm_one(r):
        have("tokens", "mix_gain")
        tok.wait(r)
        norm_rows(s.tok, s.v_mix_gain, r)

    def mix_in(r):
        if r == 0:
            have("value", "gate", "conv_taps")
            ready(0)
            ready(1)
        x = s.xn[rows_of(r), :]
        value = dot(x, s.wv[...])
        gate = dot(x, s.wg[...])
        s.glu[pl.ds(PAD + r * n.rows, n.rows), :] = value * sigmoid(gate)

    def conv(r):
        tile, half = 64, (n.taps - 1) // 2
        window = tile + 2 * PAD
        for lanes in range(0, n.own_channels, LANES):
            columns = slice(lanes, lanes + LANES)

            def body(first):
                x = s.glu[pl.ds(first, window), columns]
                total = jnp.zeros((tile, LANES), F32)
                for shift in range(8):
                    moved = pltpu.roll(x, window - shift, 0) if shift else x
                    for k in range(n.taps):
                        at = PAD - half + k
                        if at % 8 == shift:
                            piece = moved[at - shift : at - shift + tile]
                            total = total + s.v_conv_taps[k : k + 1, columns] * piece
                s.cv[tp, pl.ds(first, tile), columns] = total.astype(BF16)

            each_tile(r, tile, body)
        cv.send(r)

    def mix_result(r):
        if r == 0:
            have("chan_gain", "chan_shift", "mix")
            ready(2)
        cv.wait(r)

        def body(first):
            rows = pl.ds(first, 32)
            total = jnp.zeros((32, 1), F32)
            square = jnp.zeros((32, 1), F32)
            for t in range(n.tps):
                v = s.cv[t, rows, :].astype(F32)
                total = total + jnp.sum(v, axis=-1, keepdims=True)
                square = square + jnp.sum(v * v, axis=-1, keepdims=True)
            mean = total / n.channels
            scale = lax.rsqrt(square / n.channels - mean * mean + 1e-05)
            for t in range(n.tps):
                columns = slice(t * n.own_channels, (t + 1) * n.own_channels)
                v = s.cv[t, rows, :].astype(F32)
                v = (v - mean) * scale * s.v_chan_gain[:, columns] + s.v_chan_shift[:, columns]
                s.hm[rows, columns] = (v * sigmoid(v)).astype(BF16)

        each_tile(r, 32, body)
        rows = rows_of(r)
        result = dot(s.hm[rows, :], s.wm[...])
        s.mx[tp, rows, :] = (s.tok[tp, rows, :].astype(F32) + result).astype(BF16)
        mx.send(r)

    def norm_two(r):
        have("mlp_gain")
        mx.wait(r)
        norm_rows(s.mx, s.v_mlp_gain, r)

    def mlp_in(c, r):
        first, width = n.mlp_cols[c]
        if r == 0:
            have("mgate", "mup", "gate_taps", "up_taps")
            ready(first_mlp + 2 * c)
            ready(first_mlp + 2 * c + 1)
        x = s.xn[rows_of(r), :]
        rows = pl.ds(EDGE + r * n.rows, n.rows)
        s.gp[rows, :width] = dot(x, s.wgate[:, first : first + width])
        s.up[rows, :width] = dot(x, s.wup[:, first : first + width])

    def mlp_act(c, r):
        first_column, width = n.mlp_cols[c]
        tile = 32
        window = tile + 2 * EDGE

        def filtered(values, taps, first, lanes, columns):
            x = values[pl.ds(first, window), lanes : lanes + LANES]
            low = pltpu.roll(x, 1, 0)[EDGE : EDGE + tile]
            high = pltpu.roll(x, window - 1, 0)[EDGE : EDGE + tile]
            middle = x[EDGE : EDGE + tile]
            return taps[0:1, columns] * low + taps[1:2, columns] * middle + taps[2:3, columns] * high

        def body(first):
            for lanes in range(0, width, LANES):
                columns = slice(first_column + lanes, first_column + lanes + LANES)
                gate = filtered(s.gp, s.v_gate_taps, first, lanes, columns)
                up = filtered(s.up, s.v_up_taps, first, lanes, columns)
                s.hidden[pl.ds(first, tile), columns] = (gate * sigmoid(gate) * up).astype(BF16)

        each_tile(r, tile, body)

    own_blocks = n.cols // LANES
    pending = []

    def block_of(f, j):
        b = f * n.down_blocks + j
        owner = b // own_blocks
        return b, owner, owner % CORES

    def to_sibling(b):
        return pltpu.make_async_remote_copy(
            src_ref=s.stage.at[b],
            dst_ref=s.sib_in.at[b],
            send_sem=s.stage_send.at[b],
            recv_sem=s.sib_recv.at[b],
            device_id={"tp": sibling},
            device_id_type=MESH,
        )

    def to_owner(b, owner):
        jump = (chip - owner // CORES + n.chips) % n.chips
        index = jnp.maximum(jump - 1, 0)
        return pltpu.make_async_remote_copy(
            src_ref=s.stage.at[b],
            dst_ref=s.own_in.at[index, b % own_blocks],
            send_sem=s.stage_send.at[b],
            recv_sem=s.own_recv.at[index, b % own_blocks],
            device_id={"tp": owner},
            device_id_type=MESH,
        )

    def collect(f, j, keep):
        b, owner, side = block_of(f, j)

        @pl.when(side == core)
        def _():
            to_sibling(b).wait_recv()

            @pl.when(owner == tp)
            def _():
                for r in range(n.pieces):
                    rows = rows_of(r)
                    s.total[b % own_blocks, rows, :] = s.kept[keep, rows, :] + s.sib_in[b, rows, :].astype(F32)

            @pl.when(owner != tp)
            def _():
                for r in range(n.pieces):
                    rows = rows_of(r)
                    both = s.kept[keep, rows, :] + s.sib_in[b, rows, :].astype(F32)
                    s.stage[b, rows, :] = both.astype(BF16)
                to_owner(b, owner).start()

    def block(f, j, arrived):
        if arrived:
            wait_y(first_down + j, f)
        else:
            have("down")
        b, owner, side = block_of(f, j)
        keep = len(pending) % 2

        def step(r, carry):
            rows = pl.ds(pl.multiple_of(r * n.rows, n.rows), n.rows)
            partial = dot(s.hidden[rows, :], s.wd[f, :, j * LANES : (j + 1) * LANES])

            @pl.when(side == core)
            def _():
                s.kept[keep, rows, :] = partial

            @pl.when(side != core)
            def _():
                s.stage[b, rows, :] = partial.astype(BF16)

            return carry

        lax.fori_loop(0, n.pieces, step, 0)

        @pl.when(side != core)
        def _():
            to_sibling(b).start()

        if pending:
            collect(*pending[-1])
        pending.append((f, j, keep))

    tasks = []

    def at(position, cost, work, *args):
        tasks.append((position, cost, work, args))

    lag = 2.0 / max(last, 1)
    piece_at = [3.0 * r / n.pieces for r in range(n.pieces)]
    for r in range(n.pieces):
        at(0.6 + 2.0 * (r / n.pieces) * 4 / 3, 0.2, tok.forward, r)
        at(1.0 + 2.0 * (r / n.pieces) * 4 / 3, 1.0, norm_one, r)
    for r in range(n.pieces):
        at(3.0, 1.5, mix_in, r)
    for r in range(n.pieces):
        at(3.6, 1.5, conv, r)
    for r in range(n.pieces):
        at(4.3, 0.2, cv.forward, r)
        at(4.3, 2.0, mix_result, r)
    for r in range(n.pieces):
        at(5.3 + 0.45 * r, 0.2, mx.forward, r)
        at(5.6 + 0.45 * r, 1.0, norm_two, r)
    for c in range(len(n.mlp_cols)):
        for r in range(n.pieces):
            at(first_mlp + 2 * (c + 1) + lag, 1.2, mlp_in, c, r)
        for r in range(n.pieces):
            at(first_mlp + 2 * (c + 1) + lag, 0.6, mlp_act, c, r)
    for j in range(n.down_blocks):
        at(0, 1.2, block, fs, j, False)
    for j in range(n.down_blocks):
        for step in range(1, n.shards):
            at(first_down + j + step / max(last, 1) + lag, 1.2, block, arrival(step), j, True)
    drains = [(i + 5.0, drain_chunk, i) for i in range(n.chunks)]
    drains += [(first_down + 0.5, gather.drain, r) for gather in (tok, cv, mx) for r in range(n.pieces)]
    drains.sort(key=lambda entry: entry[0])

    def run_tasks(now, budget):
        while tasks and tasks[0][0] <= now + 1e-6 and budget > 0:
            _, cost, work, args = tasks.pop(0)
            work(*args)
            budget -= cost

    peers = [("tp", (tp + jump) % n.tps) for jump in range(1, n.tps)]
    peers += [("grp", (group + jump) % n.groups) for jump in range(1, n.groups)]
    barrier = pltpu.get_barrier_semaphore()

    def greet(axis, index):
        pl.semaphore_signal(barrier, inc=1, device_id={axis: index}, device_id_type=MESH)

    for axis, index in peers:
        greet(axis, index)

    @pl.when(fs < last)
    def _():
        greet("fs", fs + 1)

    @pl.when(fs > 0)
    def _():
        greet("fs", fs - 1)

    ends = jnp.where(fs == 0, 1, 0) + jnp.where(fs == last, 1, 0)
    pl.semaphore_wait(barrier, len(peers) + 2 - ends)

    for r in range(n.pieces):
        tok.send(r)
        if r < LEAD:
            send_own(r)
    s.glu[:PAD, :] = jnp.zeros((PAD, n.own_channels), F32)
    s.glu[PAD + n.tokens :, :] = jnp.zeros((PAD, n.own_channels), F32)
    for ref in (s.gp, s.up):
        ref[:EDGE, :] = jnp.zeros((EDGE, ref.shape[1]), F32)
        ref[EDGE + n.tokens :, :] = jnp.zeros((EDGE, ref.shape[1]), F32)

    for i in range(n.chunks):
        for step in range(1, n.shards):
            pump(i, step)
            if step == last and i + LEAD < n.chunks:
                send_own(i + LEAD)
            now = i + step / last
            run_tasks(now, BUDGET)
            if drains and drains[0][0] <= now:
                _, work, arg = drains.pop(0)
                work(arg)
    run_tasks(1e9, 1e9)
    collect(*pending[-1])

    have("final_gain")
    for jump in range(1, n.chips):
        for j in range(own_blocks):
            pltpu.make_async_remote_copy(
                src_ref=s.stage.at[0],
                dst_ref=s.own_in.at[jump - 1, j],
                send_sem=s.stage_send.at[0],
                recv_sem=s.own_recv.at[jump - 1, j],
                device_id={"tp": sibling},
                device_id_type=MESH,
            ).wait_recv()

    def sum_up(first):
        rows = pl.ds(first, LANES)
        squares = jnp.zeros((LANES, LANES), F32)
        for j in range(own_blocks):
            columns = slice(j * LANES, (j + 1) * LANES)
            v = s.total[j, rows, :] + s.mx[tp, rows, columns].astype(F32)
            for jump in range(1, n.chips):
                v = v + s.own_in[jump - 1, j, rows, :].astype(F32)
            s.total[j, rows, :] = v
            squares = squares + v * v
        across = jnp.sum(jnp.transpose(squares), axis=0, keepdims=True)
        s.stats[tp, :, rows] = jnp.broadcast_to(across, (8, LANES))

    def each_block(body):
        def step(q, carry):
            body(pl.multiple_of(q * LANES, LANES))
            return carry

        lax.fori_loop(0, n.tokens // LANES, step, 0)

    each_block(sum_up)

    def stats_copy(sender, jump):
        return pltpu.make_async_remote_copy(
            src_ref=s.stats.at[sender],
            dst_ref=s.stats.at[sender],
            send_sem=s.stats_send.at[jump - 1],
            recv_sem=s.stats_recv.at[jump - 1],
            device_id={"tp": (tp + jump) % n.tps},
            device_id_type=MESH,
        )

    for jump in range(1, n.tps):
        stats_copy(tp, jump).start()
    for _, work, arg in drains:
        work(arg)
    for b in range(n.shards * n.down_blocks):
        owner = b // own_blocks

        @pl.when(owner != tp)
        def _():
            to_sibling(b).wait_send()

    for jump in range(1, n.tps):
        stats_copy((tp - jump + n.tps) % n.tps, jump).wait_recv()

    def finish(first):
        rows = pl.ds(first, LANES)
        across = s.stats[0, 0:1, rows]
        for t in range(1, n.tps):
            across = across + s.stats[t, 0:1, rows]
        square = jnp.transpose(jnp.broadcast_to(across, (LANES, LANES)))
        scale = lax.rsqrt(square / n.width + 1e-06)
        for j in range(own_blocks):
            columns = slice(j * LANES, (j + 1) * LANES)
            out[rows, columns] = (s.total[j, rows, :] * scale * s.v_final_gain[:, columns]).astype(BF16)

    each_block(finish)
    for jump in range(1, n.tps):
        stats_copy(tp, jump).wait_send()


def wide(array, axis):
    extra = -array.shape[axis] % LANES
    if not extra:
        return array
    return jnp.pad(array, [(0, extra if k == axis else 0) for k in range(array.ndim)])


INPUTS = (
    "tokens",
    "mix_gain",
    "value",
    "gate",
    "conv_taps",
    "chan_gain",
    "chan_shift",
    "mix",
    "mlp_gain",
    "mgate",
    "mup",
    "gate_taps",
    "up_taps",
    "down",
    "final_gain",
)
SMALL = (
    "mix_gain",
    "conv_taps",
    "chan_gain",
    "chan_shift",
    "mlp_gain",
    "gate_taps",
    "up_taps",
    "final_gain",
)


def local(*values):
    a = dict(zip(INPUTS, values))
    for name in ("mix_gain", "chan_gain", "chan_shift", "mlp_gain", "final_gain"):
        a[name] = a[name][None]
    for name in ("mgate", "mup", "gate_taps", "up_taps"):
        a[name] = wide(a[name], 1)
    a["down"] = wide(a["down"], 0)
    tps, shards, groups = lax.axis_size("tp"), lax.axis_size("fs"), lax.axis_size("grp")
    chips = tps // CORES
    tokens, cols = a["tokens"].shape
    depth, own_channels = a["value"].shape
    hidden = a["mgate"].shape[1]
    mlp_cols = column_chunks(hidden, 3 * LANES)
    down_blocks = a["down"].shape[1] // LANES
    rows = min(256, tokens)
    pieces = tokens // rows
    chunks = 3 + 2 * len(mlp_cols) + down_blocks
    width, channels = cols * tps, own_channels * tps
    blocks = shards * down_blocks
    own_blocks = cols // LANES
    edge = tokens + 2 * EDGE
    vmem, dma = pltpu.VMEM, pltpu.SemaphoreType.DMA
    scratch = {
        "tok": vmem((tps, tokens, cols), BF16),
        "cv": vmem((tps, tokens, own_channels), BF16),
        "mx": vmem((tps, tokens, cols), BF16),
        "xn": vmem((tokens, width), BF16),
        "hm": vmem((tokens, channels), BF16),
        "glu": vmem((tokens + 2 * PAD, own_channels), F32),
        "gp": vmem((edge, mlp_cols[0][1]), F32),
        "up": vmem((edge, mlp_cols[0][1]), F32),
        "hidden": vmem((tokens, hidden), BF16),
        "wv": vmem((width, own_channels), BF16),
        "wg": vmem((width, own_channels), BF16),
        "wm": vmem((channels, cols), BF16),
        "wgate": vmem((width, hidden), BF16),
        "wup": vmem((width, hidden), BF16),
        "wd": vmem((shards,) + a["down"].shape, BF16),
        "kept": vmem((2, tokens, LANES), F32),
        "stage": vmem((blocks, tokens, LANES), BF16),
        "sib_in": vmem((blocks, tokens, LANES), BF16),
        "own_in": vmem((chips - 1, own_blocks, tokens, LANES), BF16),
        "total": vmem((own_blocks, tokens, LANES), F32),
        "stats": vmem((tps, 8, tokens), F32),
        "local_sem": dma((7 + len(SMALL),)),
        "z_recv": dma((chunks, shards)),
        "up_send": dma((chunks, shards)),
        "down_send": dma((chunks, shards)),
        "y_send": dma((groups - 1, chunks, shards)),
        "y_recv": dma((groups - 1, chunks, shards)),
        "gather_send": dma((3, 2 * chips - 1, pieces)),
        "gather_recv": dma((3, tps, pieces)),
        "stage_send": dma((blocks,)),
        "sib_recv": dma((blocks,)),
        "own_recv": dma((chips - 1, own_blocks)),
        "stats_send": dma((tps - 1,)),
        "stats_recv": dma((tps - 1,)),
    }
    for name in SMALL:
        scratch["v_" + name] = vmem(a[name].shape, F32)
    n = SimpleNamespace(
        inputs=INPUTS,
        small=SMALL,
        scratch=tuple(scratch),
        tps=tps,
        shards=shards,
        groups=groups,
        chips=chips,
        tokens=tokens,
        rows=rows,
        pieces=pieces,
        cols=cols,
        width=width,
        channels=channels,
        own_channels=own_channels,
        depth=depth,
        mix_depth=a["mix"].shape[0],
        hidden=hidden,
        mlp_cols=mlp_cols,
        down_blocks=down_blocks,
        chunks=chunks,
        taps=a["conv_taps"].shape[0],
    )
    return pl.pallas_call(
        functools.partial(layer_kernel, n),
        out_shape=jax.ShapeDtypeStruct((tokens, cols), BF16),
        in_specs=[pl.BlockSpec(memory_space=pl.ANY)] * len(INPUTS),
        out_specs=pl.BlockSpec(memory_space=pltpu.VMEM),
        scratch_shapes=list(scratch.values()),
        compiler_params=pltpu.CompilerParams(
            collective_id=0, has_side_effects=True, vmem_limit_bytes=67043328
        ),
        name="layer",
    )(*[a[name] for name in INPUTS])


def solution(mesh):
    return jax.shard_map(
        local,
        mesh=mesh,
        in_specs=(
            P(("grp", "fs"), "tp"),
            P(),
            P("fs", "tp"),
            P("fs", "tp"),
            P(None, "tp"),
            P(),
            P(),
            P("fs", "tp"),
            P(),
            P("fs", "tp"),
            P("fs", "tp"),
            P(None, "tp"),
            P(None, "tp"),
            P("tp", "fs"),
            P("tp"),
        ),
        out_specs=P(("grp", "fs"), "tp"),
        check_vma=False,
    )
```

profile of v0, /device:TPU:0, one launch (start us, length us, event | category | flops | bytes accessed | tf_op | source)
XLA Modules:
  0.0 210.9 jit_solution(6969865024146476884)
XLA Ops:
  0.0 208.6 %layer.1 = bf16[1024,512]{1,0:T(8,128)(2,1)} custom-call(bf16[1024,512]{1,0:T(8,128)(2,1)} %refs_0_.1, f32[1,2048]{1,0:T(1,128)} %bitcast.5, bf16[512,256]{1,0:T(8,128)(2,1)} %refs_2_.1, bf16[512,256]{1,0:T(8,128)(2,1)} %refs_3_.1, f32[31,256]{1,0:T(8,128)} %refs_4_.1, f32[1,1024]{1,0:T(1,128)} %bitcast.7, f32[1,1024]{1,0:T(1,128)} %bitcast.8, ...), custom_call_target="tpu_custom_call" | custom-call | tf_op jit(solution)/shard_map/layer/pallas_call | solution.py:722
  208.6 2.3 %copy.17 = bf16[1024,512]{1,0:T(8,128)(2,1)} copy(bf16[1024,512]{1,0:T(8,128)(2,1)} %layer.1) | data formatting | bytes 2097152
where the time goes:
time: 211 us
  Pallas kernels  209 us (99%)
  local copies, waits for them, and re-layouts  2.26 us (1%)
    pallas_call x1, Pallas kernels, local(): pl.pallas_call(functools.partial(layer_kernel, n), out_shape=jax.ShapeDty...  209 us

commit v1 on v0

--- a/solution.py
+++ b/solution.py
@@ -13,6 +13,10 @@
 LANES = 128
 CORES = 2
 LEAD = 2
+BLOCK_ROWS = 512
+WHOLE = 4
+MLP_LAG = 3
+DOWN_LAG = 2
 PAD = 16
 EDGE = 8
 BUDGET = 4.5
@@ -70,48 +74,63 @@
     load("down", arrays.down, s.wd.at[fs])
 
     chunks = [
-        (arrays.value, s.wv, n.depth, 0, n.own_channels),
-        (arrays.gate, s.wg, n.depth, 0, n.own_channels),
-        (arrays.mix, s.wm, n.mix_depth, 0, n.cols),
+        (arrays.value, s.wv, 0, n.depth, 0, n.own_channels),
+        (arrays.gate, s.wg, 0, n.depth, 0, n.own_channels),
+        (arrays.mix, s.wm, 0, n.mix_depth, 0, n.cols),
     ]
     first_mlp = len(chunks)
     for first, width in n.mlp_cols:
-        chunks.append((arrays.mgate, s.wgate, n.depth, first, width))
-        chunks.append((arrays.mup, s.wup, n.depth, first, width))
+        chunks.append((arrays.mgate, s.wgate, 0, n.depth, first, width))
+        chunks.append((arrays.mup, s.wup, 0, n.depth, first, width))
     first_down = len(chunks)
     for j in range(n.down_blocks):
-        chunks.append((arrays.down, s.wd, n.hidden, j * LANES, LANES))
+        count = n.hidden - (n.whole_rows if j == n.down_blocks - 1 else 0)
+        chunks.append((arrays.down, s.wd, 0, count, j * LANES, LANES))
+    whole = len(chunks)
+    chunks.append((arrays.down, s.wd, count, n.whole_rows, j * LANES, LANES))
     assert len(chunks) == n.chunks
+    kinds = [0, 1, 2] + [3 + i % 2 for i in range(first_down - first_mlp)]
+    kinds += [5] * (n.down_blocks - 1) + [6, 7]
+
+    def part_rows(i, part):
+        row, count = chunks[i][2:4]
+        if i == whole:
+            return row, count
+        half = count // n.groups
+        return pl.multiple_of(row + part * half, half), half
 
     def slot(i, f, part):
-        _, dst, depth, first, width = chunks[i]
-        half = depth // n.groups
+        _, dst, _, _, first, width = chunks[i]
+        row, half = part_rows(i, part)
         columns = pl.ds(first, width)
         if i >= first_down:
-            return dst.at[f, pl.ds(pl.multiple_of(part * half, half), half), columns]
-        return dst.at[pl.ds(pl.multiple_of(f * depth + part * half, half), half), columns]
+            return dst.at[f, pl.ds(row, half), columns]
+        return dst.at[pl.ds(pl.multiple_of(f * chunks[i][3] + row, half), half), columns]
 
     def z_copy(i, f, to, sems, own=False):
         src = slot(i, f, group)
         if own:
-            source, _, depth, first, width = chunks[i]
-            half = depth // n.groups
-            src = source.at[pl.ds(pl.multiple_of(group * half, half), half), pl.ds(first, width)]
+            source, _, _, _, first, width = chunks[i]
+            row, half = part_rows(i, group)
+            src = source.at[pl.ds(row, half), pl.ds(first, width)]
         return pltpu.make_async_remote_copy(
             src_ref=src,
             dst_ref=slot(i, f, group),
-            send_sem=sems.at[i, f],
+            send_sem=sems.at[kinds[i]],
             recv_sem=s.z_recv.at[i, f],
             device_id={"fs": to},
             device_id_type=MESH,
         )
 
-    def y_copy(i, f, jump, part):
+    def y_copy(i, f, jump, part, refs=None):
+        refs = slot(i, f, part) if refs is None else refs
+        down = i >= first_down
+        recv_sem = s.y_down.at[jump - 1, i - first_down, f] if down else s.y_recv.at[jump - 1, i]
         return pltpu.make_async_remote_copy(
-            src_ref=slot(i, f, part),
-            dst_ref=slot(i, f, part),
-            send_sem=s.y_send.at[jump - 1, i, f],
-            recv_sem=s.y_recv.at[jump - 1, i, f],
+            src_ref=refs,
+            dst_ref=refs,
+            send_sem=s.y_send.at[jump - 1, kinds[i]],
+            recv_sem=recv_sem,
             device_id={"grp": (group + jump) % n.groups},
             device_id_type=MESH,
         )
@@ -146,7 +165,7 @@
         def _():
             z_copy(i, f, fs - 1, s.down_send).start()
 
-        for jump in range(1, n.groups):
+        for jump in range(1, n.groups if i != whole else 1):
             y_copy(i, f, jump, group).start()
 
     def wait_y(i, f):
@@ -154,80 +173,99 @@
             y_copy(i, f, jump, (group - jump + n.groups) % n.groups).wait_recv()
 
     def ready(i):
-        for step in range(1, n.shards):
-            wait_y(i, arrival(step))
-
-    def drain_chunk(i):
-        @pl.when(fs < last)
-        def _():
-            z_copy(i, fs, fs + 1, s.up_send, own=True).wait_send()
-
-        @pl.when(fs > 0)
-        def _():
-            z_copy(i, fs, fs - 1, s.down_send, own=True).wait_send()
-
-        for step in range(1, n.shards):
-            f = arrival(step)
-
-            @pl.when(jnp.logical_and(f < fs, fs < last))
+        _, dst, _, depth, first, width = chunks[i]
+        refs = dst.at[pl.ds(0, last * (depth // n.groups)), pl.ds(first, width)]
+        for jump in range(1, n.groups):
+            y_copy(i, fs, jump, group, refs).wait_recv()
+
+    def sent(kind, count):
+        i = kinds.index(kind)
+        _, dst, _, depth, _, _ = chunks[i]
+        half = depth if kind == 7 else depth // n.groups
+        if kind < 5:
+            return i, dst.at[pl.ds(0, count * half), :]
+        columns = (n.down_blocks - 1 if kind == 5 else 1) * LANES
+        return i, dst.at[pl.ds(0, count), pl.ds(0, half), pl.ds(0, columns)]
+
+    def drain():
+        def wait(sems, to, count, kind):
+            i, refs = sent(kind, count)
+            pltpu.make_async_remote_copy(
+                src_ref=refs,
+                dst_ref=refs,
+                send_sem=sems.at[kind],
+                recv_sem=s.z_recv.at[0, 0],
+                device_id={"fs": to},
+                device_id_type=MESH,
+            ).wait_send()
+
+        used = sorted(set(kinds))
+        for count in range(1, n.shards):
+
+            @pl.when(fs + 1 == count)
             def _():
-                z_copy(i, f, fs + 1, s.up_send).wait_send()
-
-            @pl.when(jnp.logical_and(f > fs, fs > 0))
+                for kind in used:
+                    wait(s.up_send, fs + 1, count, kind)
+
+            @pl.when(last - fs + 1 == count)
             def _():
-                z_copy(i, f, fs - 1, s.down_send).wait_send()
-
+                for kind in used:
+                    wait(s.down_send, fs - 1, count, kind)
+
+        for kind in used[:-1]:
+            i, refs = sent(kind, last)
             for jump in range(1, n.groups):
-                y_copy(i, f, jump, group).wait_send()
+                y_copy(i, fs, jump, group, refs).wait_send()
 
     class Gather:
         def __init__(self, blocks, kind, own=None):
             self.blocks, self.kind, self.own = blocks, kind, own
 
-        def copy(self, block, r, to, send, src=None):
+        def copy(self, block, r, to, jump, src=None):
             dst = self.blocks.at[block, rows_of(r), :]
+            sems = s.gather_chip.at[self.kind, jump - 1, r] if jump else s.gather_core.at[self.kind, r]
             return pltpu.make_async_remote_copy(
                 src_ref=dst if src is None else src,
                 dst_ref=dst,
-                send_sem=s.gather_send.at[self.kind, send, r],
-                recv_sem=s.gather_recv.at[self.kind, block, r],
+                send_sem=s.gather_send.at[self.kind],
+                recv_sem=sems,
                 device_id={"tp": to},
                 device_id_type=MESH,
             )
 
-        def own_copies(self, r):
+        def send(self, r):
             src = None if self.own is None else self.own.at[rows_of(r), :]
-            copies = [
-                self.copy(tp, r, chip_at(jump) * CORES + core, jump, src)
-                for jump in range(1, n.chips)
-            ]
-            return copies + [self.copy(tp, r, sibling, 0, src)]
-
-        def passed(self, r, jump):
-            block = chip_at(-jump) * CORES + core
-            return self.copy(block, r, sibling, n.chips - 1 + jump)
-
-        def send(self, r):
-            for copy in self.own_copies(r):
-                copy.start()
+            for jump in range(1, n.chips):
+                self.copy(tp, r, chip_at(jump) * CORES + core, jump, src).start()
+            self.copy(tp, r, sibling, 0, src).start()
 
         def forward(self, r):
             for jump in range(1, n.chips):
-                copy = self.passed(r, jump)
-                copy.wait_recv()
-                copy.start()
+                block = chip_at(-jump) * CORES + core
+                self.copy(block, r, sibling, jump).wait_recv()
+                self.copy(block, r, sibling, 0).start()
 
         def wait(self, r):
-            self.copy(sibling, r, sibling, 0).wait_recv()
-            for jump in range(1, n.chips):
-                block = chip_at(-jump) * CORES + 1 - core
-                self.copy(block, r, sibling, 0).wait_recv()
-
-        def drain(self, r):
-            for copy in self.own_copies(r):
-                copy.wait_send()
-            for jump in range(1, n.chips):
-                self.passed(r, jump).wait_send()
+            refs = self.blocks.at[pl.ds(0, n.chips), rows_of(r), :]
+            pltpu.make_async_remote_copy(
+                src_ref=refs,
+                dst_ref=refs,
+                send_sem=s.gather_send.at[self.kind],
+                recv_sem=s.gather_core.at[self.kind, r],
+                device_id={"tp": sibling},
+                device_id_type=MESH,
+            ).wait_recv()
+
+        def drain(self):
+            refs = self.blocks.at[pl.ds(0, 2 * n.chips - 1)]
+            pltpu.make_async_remote_copy(
+                src_ref=refs,
+                dst_ref=refs,
+                send_sem=s.gather_send.at[self.kind],
+                recv_sem=s.gather_core.at[self.kind, 0],
+                device_id={"tp": sibling},
+                device_id_type=MESH,
+            ).wait_send()
 
     tok = Gather(s.tok, 0, arrays.tokens)
     cv = Gather(s.cv, 1)
@@ -367,60 +405,77 @@
         owner = b // own_blocks
         return b, owner, owner % CORES
 
-    def to_sibling(b):
+    def sib_index(b):
+        return b // own_blocks // CORES * own_blocks + b % own_blocks
+
+    def block_rows(r):
+        return pl.ds(pl.multiple_of(r * n.block_rows, n.block_rows), n.block_rows)
+
+    def to_sibling(b, r):
         return pltpu.make_async_remote_copy(
-            src_ref=s.stage.at[b],
-            dst_ref=s.sib_in.at[b],
-            send_sem=s.stage_send.at[b],
-            recv_sem=s.sib_recv.at[b],
+            src_ref=s.stage.at[b, block_rows(r)],
+            dst_ref=s.sib_in.at[sib_index(b), block_rows(r)],
+            send_sem=s.stage_send.at[0],
+            recv_sem=s.sib_recv.at[sib_index(b), r],
             device_id={"tp": sibling},
             device_id_type=MESH,
         )
 
-    def to_owner(b, owner):
-        jump = (chip - owner // CORES + n.chips) % n.chips
-        index = jnp.maximum(jump - 1, 0)
+    def to_owner(b, r, owner, index):
         return pltpu.make_async_remote_copy(
-            src_ref=s.stage.at[b],
-            dst_ref=s.own_in.at[index, b % own_blocks],
-            send_sem=s.stage_send.at[b],
-            recv_sem=s.own_recv.at[index, b % own_blocks],
+            src_ref=s.stage.at[b, block_rows(r)],
+            dst_ref=s.own_in.at[index, b % own_blocks, block_rows(r)],
+            send_sem=s.stage_send.at[0],
+            recv_sem=s.own_recv.at[index, b % own_blocks, r],
             device_id={"tp": owner},
             device_id_type=MESH,
         )
 
+    def each_piece(body):
+        def step(r, carry):
+            body(r, block_rows(r))
+            return carry
+
+        lax.fori_loop(0, n.tokens // n.block_rows, step, 0)
+
     def collect(f, j, keep):
         b, owner, side = block_of(f, j)
-
-        @pl.when(side == core)
+        jump = (chip - owner // CORES + n.chips) % n.chips
+        index = jnp.maximum(jump - 1, 0)
+
+        @pl.when(jnp.logical_and(side == core, owner == tp))
         def _():
-            to_sibling(b).wait_recv()
-
-            @pl.when(owner == tp)
-            def _():
-                for r in range(n.pieces):
-                    rows = rows_of(r)
-                    s.total[b % own_blocks, rows, :] = s.kept[keep, rows, :] + s.sib_in[b, rows, :].astype(F32)
-
-            @pl.when(owner != tp)
-            def _():
-                for r in range(n.pieces):
-                    rows = rows_of(r)
-                    both = s.kept[keep, rows, :] + s.sib_in[b, rows, :].astype(F32)
-                    s.stage[b, rows, :] = both.astype(BF16)
-                to_owner(b, owner).start()
-
-    def block(f, j, arrived):
-        if arrived:
+            def body(r, rows):
+                to_sibling(b, r).wait_recv()
+                s.total[b % own_blocks, rows, :] = s.kept[keep, rows, :] + s.sib_in[sib_index(b), rows, :].astype(F32)
+
+            each_piece(body)
+
+        @pl.when(jnp.logical_and(side == core, owner != tp))
+        def _():
+            def body(r, rows):
+                to_sibling(b, r).wait_recv()
+                both = s.kept[keep, rows, :] + s.sib_in[sib_index(b), rows, :].astype(F32)
+                s.stage[b, rows, :] = both.astype(BF16)
+                to_owner(b, r, owner, index).start()
+
+            each_piece(body)
+
+    def block(f, j, step):
+        last_columns = j == n.down_blocks - 1
+        if step == 0:
+            have("down")
+        elif not last_columns:
             wait_y(first_down + j, f)
-        else:
-            have("down")
         b, owner, side = block_of(f, j)
         keep = len(pending) % 2
-
-        def step(r, carry):
-            rows = pl.ds(pl.multiple_of(r * n.rows, n.rows), n.rows)
-            partial = dot(s.hidden[rows, :], s.wd[f, :, j * LANES : (j + 1) * LANES])
+        columns = slice(j * LANES, (j + 1) * LANES)
+
+        def body(r, rows):
+            if step and last_columns:
+                partial = s.early[step - 1, rows, :] + dot(s.hidden[rows, count:], s.wd[f, count:, columns])
+            else:
+                partial = dot(s.hidden[rows, :], s.wd[f, :, columns])
 
             @pl.when(side == core)
             def _():
@@ -429,26 +484,30 @@
             @pl.when(side != core)
             def _():
                 s.stage[b, rows, :] = partial.astype(BF16)
-
-            return carry
-
-        lax.fori_loop(0, n.pieces, step, 0)
-
-        @pl.when(side != core)
-        def _():
-            to_sibling(b).start()
-
+                to_sibling(b, r).start()
+
+        each_piece(body)
         if pending:
             collect(*pending[-1])
         pending.append((f, j, keep))
 
+    def early(f, j, step):
+        wait_y(first_down + j, f)
+        columns = slice(j * LANES, (j + 1) * LANES)
+
+        def body(r, rows):
+            s.early[step - 1, rows, :] = dot(s.hidden[rows, :count], s.wd[f, :count, columns])
+
+        each_piece(body)
+
     tasks = []
 
     def at(position, cost, work, *args):
         tasks.append((position, cost, work, args))
 
-    lag = 2.0 / max(last, 1)
-    piece_at = [3.0 * r / n.pieces for r in range(n.pieces)]
+    def beats(count):
+        return count / max(last, 1)
+
     for r in range(n.pieces):
         at(0.6 + 2.0 * (r / n.pieces) * 4 / 3, 0.2, tok.forward, r)
         at(1.0 + 2.0 * (r / n.pieces) * 4 / 3, 1.0, norm_one, r)
@@ -457,25 +516,25 @@
     for r in range(n.pieces):
         at(3.6, 1.5, conv, r)
     for r in range(n.pieces):
-        at(4.3, 0.2, cv.forward, r)
-        at(4.3, 2.0, mix_result, r)
+        at(4.3 + 0.33 * r, 0.2, cv.forward, r)
+        at(4.6 + 0.33 * r, 4.0, mix_result, r)
     for r in range(n.pieces):
-        at(5.3 + 0.45 * r, 0.2, mx.forward, r)
-        at(5.6 + 0.45 * r, 1.0, norm_two, r)
+        at(5.6 + 0.45 * r, 0.2, mx.forward, r)
+        at(5.9 + 0.45 * r, 1.0, norm_two, r)
     for c in range(len(n.mlp_cols)):
+        ready_at = first_mlp + 2 * (c + 1) + beats(n.mlp_lag)
         for r in range(n.pieces):
-            at(first_mlp + 2 * (c + 1) + lag, 1.2, mlp_in, c, r)
+            at(ready_at, 1.2, mlp_in, c, r)
         for r in range(n.pieces):
-            at(first_mlp + 2 * (c + 1) + lag, 0.6, mlp_act, c, r)
+            at(ready_at, 0.6, mlp_act, c, r)
     for j in range(n.down_blocks):
-        at(0, 1.2, block, fs, j, False)
+        at(0, 1.2, block, fs, j, 0)
     for j in range(n.down_blocks):
+        work = block if j < n.down_blocks - 1 else early
         for step in range(1, n.shards):
-            at(first_down + j + step / max(last, 1) + lag, 1.2, block, arrival(step), j, True)
-    drains = [(i + 5.0, drain_chunk, i) for i in range(n.chunks)]
-    drains += [(first_down + 0.5, gather.drain, r) for gather in (tok, cv, mx) for r in range(n.pieces)]
-    drains.sort(key=lambda entry: entry[0])
-
+            at(first_down + j + beats(step + n.down_lag), 1.2, work, arrival(step), j, step)
+    for step in range(1, n.shards):
+        at(whole + beats(step), 1.2, block, arrival(step), j, step)
     def run_tasks(now, budget):
         while tasks and tasks[0][0] <= now + 1e-6 and budget > 0:
             _, cost, work, args = tasks.pop(0)
@@ -513,30 +572,28 @@
         ref[:EDGE, :] = jnp.zeros((EDGE, ref.shape[1]), F32)
         ref[EDGE + n.tokens :, :] = jnp.zeros((EDGE, ref.shape[1]), F32)
 
+    at_end = reach == 0
+
+    def pump_own(i):
+        pump(i, 1)
+
+    for i in range(min(LEAD, n.chunks)):
+        pl.when(at_end)(functools.partial(pump_own, i))
     for i in range(n.chunks):
-        for step in range(1, n.shards):
+        pl.when(jnp.logical_not(at_end))(functools.partial(pump_own, i))
+        run_tasks(i + 1 / last, BUDGET)
+        for step in range(2, n.shards):
             pump(i, step)
-            if step == last and i + LEAD < n.chunks:
-                send_own(i + LEAD)
-            now = i + step / last
-            run_tasks(now, BUDGET)
-            if drains and drains[0][0] <= now:
-                _, work, arg = drains.pop(0)
-                work(arg)
+            if step < last:
+                run_tasks(i + step / last, BUDGET)
+        if i + LEAD < n.chunks:
+            send_own(i + LEAD)
+            pl.when(at_end)(functools.partial(pump_own, i + LEAD))
+        run_tasks(i + 1.0, BUDGET)
     run_tasks(1e9, 1e9)
     collect(*pending[-1])
 
     have("final_gain")
-    for jump in range(1, n.chips):
-        for j in range(own_blocks):
-            pltpu.make_async_remote_copy(
-                src_ref=s.stage.at[0],
-                dst_ref=s.own_in.at[jump - 1, j],
-                send_sem=s.stage_send.at[0],
-                recv_sem=s.own_recv.at[jump - 1, j],
-                device_id={"tp": sibling},
-                device_id_type=MESH,
-            ).wait_recv()
 
     def sum_up(first):
         rows = pl.ds(first, LANES)
@@ -551,6 +608,13 @@
         across = jnp.sum(jnp.transpose(squares), axis=0, keepdims=True)
         s.stats[tp, :, rows] = jnp.broadcast_to(across, (8, LANES))
 
+    def sum_piece(r, rows):
+        for jump in range(1, n.chips):
+            for j in range(own_blocks):
+                to_owner(j, r, sibling, jump - 1).wait_recv()
+        for first in range(0, n.block_rows, LANES):
+            sum_up(pl.multiple_of(r * n.block_rows + first, LANES))
+
     def each_block(body):
         def step(q, carry):
             body(pl.multiple_of(q * LANES, LANES))
@@ -558,31 +622,34 @@
 
         lax.fori_loop(0, n.tokens // LANES, step, 0)
 
-    each_block(sum_up)
-
-    def stats_copy(sender, jump):
+    each_piece(sum_piece)
+
+    def stats_copy(refs, jump):
         return pltpu.make_async_remote_copy(
-            src_ref=s.stats.at[sender],
-            dst_ref=s.stats.at[sender],
-            send_sem=s.stats_send.at[jump - 1],
-            recv_sem=s.stats_recv.at[jump - 1],
+            src_ref=refs,
+            dst_ref=refs,
+            send_sem=s.stats_send.at[0],
+            recv_sem=s.stats_recv.at[0],
             device_id={"tp": (tp + jump) % n.tps},
             device_id_type=MESH,
         )
 
     for jump in range(1, n.tps):
-        stats_copy(tp, jump).start()
-    for _, work, arg in drains:
-        work(arg)
-    for b in range(n.shards * n.down_blocks):
-        owner = b // own_blocks
-
-        @pl.when(owner != tp)
-        def _():
-            to_sibling(b).wait_send()
-
-    for jump in range(1, n.tps):
-        stats_copy((tp - jump + n.tps) % n.tps, jump).wait_recv()
+        stats_copy(s.stats.at[tp], jump).start()
+    drain()
+    for gather in (tok, cv, mx):
+        gather.drain()
+    refs = s.stage.at[pl.ds(0, n.shards * n.down_blocks - own_blocks)]
+    pltpu.make_async_remote_copy(
+        src_ref=refs,
+        dst_ref=refs,
+        send_sem=s.stage_send.at[0],
+        recv_sem=s.stats_recv.at[0],
+        device_id={"tp": sibling},
+        device_id_type=MESH,
+    ).wait_send()
+    all_stats = s.stats.at[pl.ds(0, n.tps - 1)]
+    stats_copy(all_stats, 1).wait_recv()
 
     def finish(first):
         rows = pl.ds(first, LANES)
@@ -596,8 +663,7 @@
             out[rows, columns] = (s.total[j, rows, :] * scale * s.v_final_gain[:, columns]).astype(BF16)
 
     each_block(finish)
-    for jump in range(1, n.tps):
-        stats_copy(tp, jump).wait_send()
+    stats_copy(all_stats, 1).wait_send()
 
 
 def wide(array, axis):
@@ -652,7 +718,9 @@
     down_blocks = a["down"].shape[1] // LANES
     rows = min(256, tokens)
     pieces = tokens // rows
-    chunks = 3 + 2 * len(mlp_cols) + down_blocks
+    block_rows = min(BLOCK_ROWS, tokens)
+    chunks = 4 + 2 * len(mlp_cols) + down_blocks
+    whole_rows = hidden * WHOLE // 8 // LANES * LANES
     width, channels = cols * tps, own_channels * tps
     blocks = shards * down_blocks
     own_blocks = cols // LANES
@@ -674,25 +742,28 @@
         "wgate": vmem((width, hidden), BF16),
         "wup": vmem((width, hidden), BF16),
         "wd": vmem((shards,) + a["down"].shape, BF16),
+        "early": vmem((shards - 1, tokens, LANES), F32),
         "kept": vmem((2, tokens, LANES), F32),
         "stage": vmem((blocks, tokens, LANES), BF16),
-        "sib_in": vmem((blocks, tokens, LANES), BF16),
+        "sib_in": vmem((blocks // CORES, tokens, LANES), BF16),
         "own_in": vmem((chips - 1, own_blocks, tokens, LANES), BF16),
         "total": vmem((own_blocks, tokens, LANES), F32),
         "stats": vmem((tps, 8, tokens), F32),
         "local_sem": dma((7 + len(SMALL),)),
         "z_recv": dma((chunks, shards)),
-        "up_send": dma((chunks, shards)),
-        "down_send": dma((chunks, shards)),
-        "y_send": dma((groups - 1, chunks, shards)),
-        "y_recv": dma((groups - 1, chunks, shards)),
-        "gather_send": dma((3, 2 * chips - 1, pieces)),
-        "gather_recv": dma((3, tps, pieces)),
-        "stage_send": dma((blocks,)),
-        "sib_recv": dma((blocks,)),
-        "own_recv": dma((chips - 1, own_blocks)),
-        "stats_send": dma((tps - 1,)),
-        "stats_recv": dma((tps - 1,)),
+        "up_send": dma((8,)),
+        "down_send": dma((8,)),
+        "y_send": dma((groups - 1, 8)),
+        "y_recv": dma((groups - 1, chunks - down_blocks - 1)),
+        "y_down": dma((groups - 1, down_blocks, shards)),
+        "gather_send": dma((3,)),
+        "gather_chip": dma((3, chips - 1, pieces)),
+        "gather_core": dma((3, pieces)),
+        "stage_send": dma((1,)),
+        "sib_recv": dma((blocks // CORES, tokens // block_rows)),
+        "own_recv": dma((chips - 1, own_blocks, tokens // block_rows)),
+        "stats_send": dma((1,)),
+        "stats_recv": dma((1,)),
     }
     for name in SMALL:
         scratch["v_" + name] = vmem(a[name].shape, F32)
@@ -707,6 +778,7 @@
         tokens=tokens,
         rows=rows,
         pieces=pieces,
+        block_rows=block_rows,
         cols=cols,
         width=width,
         channels=channels,
@@ -716,6 +788,9 @@
         hidden=hidden,
         mlp_cols=mlp_cols,
         down_blocks=down_blocks,
+        whole_rows=whole_rows,
+        mlp_lag=MLP_LAG,
+        down_lag=DOWN_LAG,
         chunks=chunks,
         taps=a["conv_taps"].shape[0],
     )

time: 211 us -> 199 us (0.943)
  Pallas kernels: 209 us -> 196 us
    pallas_call x1, Pallas kernels: 209 us -> 196 us  [local(): pl.pallas_call(functools.partial(layer_kernel, n), out_shape=jax.ShapeDty...]
where the time goes in v1:
time: 199 us
  Pallas kernels  196 us (98%)
  local copies, waits for them, and re-layouts  2.26 us (1%)
    pallas_call x1, Pallas kernels, local(): pl.pallas_call(functools.partial(layer_kernel, n), out_shape=jax.ShapeDty...  196 us

profile of v1, /device:TPU:0, one launch (start us, length us, event | category | flops | bytes accessed | tf_op | source)
XLA Modules:
  0.0 198.7 jit_solution(15252884042942045535)
XLA Ops:
  0.0 196.4 %layer.1 = bf16[1024,512]{1,0:T(8,128)(2,1)} custom-call(bf16[1024,512]{1,0:T(8,128)(2,1)} %refs_0_.1, f32[1,2048]{1,0:T(1,128)} %bitcast.5, bf16[512,256]{1,0:T(8,128)(2,1)} %refs_2_.1, bf16[512,256]{1,0:T(8,128)(2,1)} %refs_3_.1, f32[31,256]{1,0:T(8,128)} %refs_4_.1, f32[1,1024]{1,0:T(1,128)} %bitcast.7, f32[1,1024]{1,0:T(1,128)} %bitcast.8, ...), custom_call_target="tpu_custom_call" | custom-call | tf_op jit(solution)/shard_map/layer/pallas_call | solution.py:797
  196.4 2.3 %copy.17 = bf16[1024,512]{1,0:T(8,128)(2,1)} copy(bf16[1024,512]{1,0:T(8,128)(2,1)} %layer.1) | data formatting | bytes 2097152

commit v2 on v1

--- a/solution.py
+++ b/solution.py
@@ -14,9 +14,11 @@
 CORES = 2
 LEAD = 2
 BLOCK_ROWS = 512
+GRANT = 67043328
 WHOLE = 4
-MLP_LAG = 3
-DOWN_LAG = 2
+MLP_LAG = 4
+DOWN_LAG = 3
+OWN_AHEAD = 5
 PAD = 16
 EDGE = 8
 BUDGET = 4.5
@@ -398,7 +400,7 @@
         each_tile(r, tile, body)
 
     own_blocks = n.cols // LANES
-    pending = []
+    pending, settled = [], []
 
     def block_of(f, j):
         b = f * n.down_blocks + j
@@ -461,6 +463,11 @@
 
             each_piece(body)
 
+    def settle():
+        if len(settled) < len(pending):
+            collect(*pending[-1])
+            settled.append(pending[-1])
+
     def block(f, j, step):
         last_columns = j == n.down_blocks - 1
         if step == 0:
@@ -487,11 +494,11 @@
                 to_sibling(b, r).start()
 
         each_piece(body)
-        if pending:
-            collect(*pending[-1])
+        settle()
         pending.append((f, j, keep))
 
     def early(f, j, step):
+        settle()
         wait_y(first_down + j, f)
         columns = slice(j * LANES, (j + 1) * LANES)
 
@@ -522,19 +529,25 @@
         at(5.6 + 0.45 * r, 0.2, mx.forward, r)
         at(5.9 + 0.45 * r, 1.0, norm_two, r)
     for c in range(len(n.mlp_cols)):
-        ready_at = first_mlp + 2 * (c + 1) + beats(n.mlp_lag)
+        final = c == len(n.mlp_cols) - 1
+        ready_at = first_mlp + 2 * (c + 1) + beats(n.mlp_lag - (1 if final else 0))
         for r in range(n.pieces):
             at(ready_at, 1.2, mlp_in, c, r)
         for r in range(n.pieces):
             at(ready_at, 0.6, mlp_act, c, r)
+    own = 0
     for j in range(n.down_blocks):
-        at(0, 1.2, block, fs, j, 0)
-    for j in range(n.down_blocks):
-        work = block if j < n.down_blocks - 1 else early
+        final = j == n.down_blocks - 1
         for step in range(1, n.shards):
-            at(first_down + j + beats(step + n.down_lag), 1.2, work, arrival(step), j, step)
-    for step in range(1, n.shards):
-        at(whole + beats(step), 1.2, block, arrival(step), j, step)
+            f = arrival(step)
+            while own < n.down_blocks and own * OWN_AHEAD <= j * 2 * last + 2 * step - 2:
+                at(0, 1.2, block, fs, own, 0)
+                own += 1
+            at(first_down + j + beats(step + n.down_lag), 1.2, early if final else block, f, j, step)
+            if final:
+                at(whole + beats(step), 1.2, block, f, j, step)
+    assert own == n.down_blocks
+
     def run_tasks(now, budget):
         while tasks and tasks[0][0] <= now + 1e-6 and budget > 0:
             _, cost, work, args = tasks.pop(0)
@@ -591,7 +604,7 @@
             pl.when(at_end)(functools.partial(pump_own, i + LEAD))
         run_tasks(i + 1.0, BUDGET)
     run_tasks(1e9, 1e9)
-    collect(*pending[-1])
+    settle()
 
     have("final_gain")
 
@@ -660,9 +673,12 @@
         scale = lax.rsqrt(square / n.width + 1e-06)
         for j in range(own_blocks):
             columns = slice(j * LANES, (j + 1) * LANES)
-            out[rows, columns] = (s.total[j, rows, :] * scale * s.v_final_gain[:, columns]).astype(BF16)
+            s.result[rows, columns] = (s.total[j, rows, :] * scale * s.v_final_gain[:, columns]).astype(BF16)
+
+        pltpu.make_async_copy(s.result.at[rows, :], out.at[rows, :], s.out_sem.at[0]).start()
 
     each_block(finish)
+    pltpu.make_async_copy(s.result, out, s.out_sem.at[0]).wait()
     stats_copy(all_stats, 1).wait_send()
 
 
@@ -749,6 +765,8 @@
         "own_in": vmem((chips - 1, own_blocks, tokens, LANES), BF16),
         "total": vmem((own_blocks, tokens, LANES), F32),
         "stats": vmem((tps, 8, tokens), F32),
+        "result": vmem((tokens, cols), BF16),
+        "out_sem": dma((1,)),
         "local_sem": dma((7 + len(SMALL),)),
         "z_recv": dma((chunks, shards)),
         "up_send": dma((8,)),
@@ -798,10 +816,10 @@
         functools.partial(layer_kernel, n),
         out_shape=jax.ShapeDtypeStruct((tokens, cols), BF16),
         in_specs=[pl.BlockSpec(memory_space=pl.ANY)] * len(INPUTS),
-        out_specs=pl.BlockSpec(memory_space=pltpu.VMEM),
+        out_specs=pl.BlockSpec(memory_space=pl.ANY),
         scratch_shapes=list(scratch.values()),
         compiler_params=pltpu.CompilerParams(
-            collective_id=0, has_side_effects=True, vmem_limit_bytes=67043328
+            collective_id=0, has_side_effects=True, vmem_limit_bytes=GRANT
         ),
         name="layer",
     )(*[a[name] for name in INPUTS])

time: 199 us -> 195 us (0.980)
  Pallas kernels: 196 us -> 193 us
    pallas_call x1, Pallas kernels: 196 us -> 193 us  [local(): pl.pallas_call(functools.partial(layer_kernel, n), out_shape=jax.ShapeDty...]
where the time goes in v2:
time: 195 us
  Pallas kernels  193 us (99%)
  local copies, waits for them, and re-layouts  2.26 us (1%)
    pallas_call x1, Pallas kernels, local(): pl.pallas_call(functools.partial(layer_kernel, n), out_shape=jax.ShapeDty...  193 us

profile of v2, /device:TPU:0, one launch (start us, length us, event | category | flops | bytes accessed | tf_op | source)
XLA Modules:
  0.0 195.3 jit_solution(7628751495671617360)
XLA Ops:
  0.0 193.0 %layer.1 = bf16[1024,512]{1,0:T(8,128)(2,1)} custom-call(bf16[1024,512]{1,0:T(8,128)(2,1)} %refs_0_.1, f32[1,2048]{1,0:T(1,128)} %bitcast.5, bf16[512,256]{1,0:T(8,128)(2,1)} %refs_2_.1, bf16[512,256]{1,0:T(8,128)(2,1)} %refs_3_.1, f32[31,256]{1,0:T(8,128)} %refs_4_.1, f32[1,1024]{1,0:T(1,128)} %bitcast.7, f32[1,1024]{1,0:T(1,128)} %bitcast.8, ...), custom_call_target="tpu_custom_call" | custom-call | tf_op jit(solution)/shard_map/layer/pallas_call | solution.py:815
  193.1 2.3 %copy.17 = bf16[1024,512]{1,0:T(8,128)(2,1)} copy(bf16[1024,512]{1,0:T(8,128)(2,1)} %layer.1) | data formatting | bytes 2097152

commit v3 on v2

--- a/solution.py
+++ b/solution.py
@@ -21,7 +21,7 @@
 OWN_AHEAD = 5
 PAD = 16
 EDGE = 8
-BUDGET = 4.5
+BUDGET = 3.4
 
 
 def column_chunks(width, most):
@@ -601,8 +601,9 @@
                 run_tasks(i + step / last, BUDGET)
         if i + LEAD < n.chunks:
             send_own(i + LEAD)
+        run_tasks(i + 1.0, BUDGET)
+        if i + LEAD < n.chunks:
             pl.when(at_end)(functools.partial(pump_own, i + LEAD))
-        run_tasks(i + 1.0, BUDGET)
     run_tasks(1e9, 1e9)
     settle()
 

time: 195 us -> 194 us (level)
  no operation moved by 1% of the time
where the time goes in v3:
time: 194 us
  Pallas kernels  192 us (99%)
  local copies, waits for them, and re-layouts  2.26 us (1%)
    pallas_call x1, Pallas kernels, local(): pl.pallas_call(functools.partial(layer_kernel, n), out_shape=jax.ShapeDty...  192 us

profile of v3, /device:TPU:0, one launch (start us, length us, event | category | flops | bytes accessed | tf_op | source)
XLA Modules:
  0.0 194.1 jit_solution(14499280094259022922)
XLA Ops:
  0.0 191.8 %layer.1 = bf16[1024,512]{1,0:T(8,128)(2,1)} custom-call(bf16[1024,512]{1,0:T(8,128)(2,1)} %refs_0_.1, f32[1,2048]{1,0:T(1,128)} %bitcast.5, bf16[512,256]{1,0:T(8,128)(2,1)} %refs_2_.1, bf16[512,256]{1,0:T(8,128)(2,1)} %refs_3_.1, f32[31,256]{1,0:T(8,128)} %refs_4_.1, f32[1,1024]{1,0:T(1,128)} %bitcast.7, f32[1,1024]{1,0:T(1,128)} %bitcast.8, ...), custom_call_target="tpu_custom_call" | custom-call | tf_op jit(solution)/shard_map/layer/pallas_call | solution.py:816
  191.9 2.3 %copy.17 = bf16[1024,512]{1,0:T(8,128)(2,1)} copy(bf16[1024,512]{1,0:T(8,128)(2,1)} %layer.1) | data formatting | bytes 2097152
